TPU v7x, 32 devices: a whole 2x2x4 slice. The times are simulated.
32 devices in a mesh: sp: 4 (over z), fs: 4 (over y, x), tp: 2 (over core).
Axes of the slice: x: 2, y: 2, z: 4, core: 2. Of those that a mesh axis runs over, the one named last changes fastest.
Arguments:
- tokens: bfloat16 [4, 512, 2048], P('fs', ('sp', 'tp')), may hold values from -6 to 6
- norm_gain: float32 [2048], replicated, may hold values from 0.1 to 1.9
- gla_query_weight: bfloat16 [2048, 512], P('sp', 'tp'), may hold values from -0.125 to 0.125
- gla_key_weight: bfloat16 [2048, 512], P('sp', 'tp'), may hold values from -0.125 to 0.125
- gla_value_weight: bfloat16 [2048, 1024], P('sp', 'tp'), may hold values from -0.125 to 0.125
- decay_down: bfloat16 [2048, 32], P('sp'), may hold values from -0.125 to 0.125
- decay_up: bfloat16 [32, 512], P(None, 'tp'), may hold values from -1 to 1
- decay_bias: float32 [512], P('tp'), may hold values from 0.5 to 12
- head_gain: float32 [128], replicated, may hold values from 0.1 to 1.9
- window_query_weight: bfloat16 [2048, 1024], P('sp', 'tp'), may hold values from -3 to 3
- window_key_weight: bfloat16 [2048, 256], P('sp', 'tp'), may hold values from -3 to 3
- window_value_weight: bfloat16 [2048, 256], P('sp', 'tp'), may hold values from -0.125 to 0.125
- sink_logit: float32 [16], P('tp'), may hold values from 3 to 7
- gla_output_weight: bfloat16 [1024, 2048], P('tp', 'sp'), may hold values from -0.125 to 0.125
- window_output_weight: bfloat16 [1024, 2048], P('tp', 'sp'), may hold values from -0.125 to 0.125
Outputs:
- mixed: bfloat16 [4, 512, 2048], P('fs', ('sp', 'tp'))
All inputs are finite; a program needn't handle non-finite values.
Results may differ from a plain program's by a relative error of at most 0.013.
Values may be sent and summed in bfloat16 or wider, within the bound.
A program may use at most 64 MiB of HBM per device.

v0:
```python
import jax
import jax.numpy as jnp
from jax import lax
from jax.sharding import PartitionSpec as P

KEY_DIM = 64
VALUE_DIM = 128
SWA_HEADS = 16
KV_HEADS = 4
HEAD_DIM = 64
WINDOW = 128
SPAN = 64
EPS = 1e-06
SOFTMAX_TEMPER = 16.0
BF = jnp.bfloat16
F32 = jnp.float32


def rms_rows(values, gain):
    mean_square = jnp.mean(values * values, axis=-1, keepdims=True)
    return values * lax.rsqrt(mean_square + EPS) * gain


def quarter(weight, along):
    width = weight.shape[along] // lax.axis_size("fs")
    return lax.dynamic_slice_in_dim(weight, lax.axis_index("fs") * width, width, along)


def shared(weight, heads):
    group = SWA_HEADS // KV_HEADS
    first = lax.axis_index("fs") * heads // group
    count = max(1, heads // group)
    return lax.dynamic_slice_in_dim(weight, first * HEAD_DIM, count * HEAD_DIM, 1)


def dot(spec, a, b):
    return jnp.einsum(spec, a.astype(BF), b.astype(BF), preferred_element_type=F32)


def per_device(
    tokens,
    norm_gain,
    gla_query_weight,
    gla_key_weight,
    gla_value_weight,
    decay_down,
    decay_up,
    decay_bias,
    head_gain,
    window_query_weight,
    window_key_weight,
    window_value_weight,
    sink_logit,
    gla_output_weight,
    window_output_weight,
):
    fs, tp, sp = (lax.axis_size(n) for n in ("fs", "tp", "sp"))
    me = lax.axis_index("sp")
    heads = sink_logit.shape[0] // fs
    maps = [
        quarter(gla_value_weight, 1),
        quarter(window_query_weight, 1),
        quarter(gla_query_weight, 1),
        quarter(gla_key_weight, 1),
        shared(window_key_weight, heads),
        shared(window_value_weight, heads),
        decay_down,
    ]
    widths = [m.shape[1] for m in maps]
    w_in = lax.all_gather(jnp.concatenate(maps, 1), "sp", axis=0, tiled=True)
    w_out = lax.all_gather(
        jnp.concatenate([quarter(gla_output_weight, 0), quarter(window_output_weight, 0)], 0), "sp"
    )
    normed = rms_rows(tokens[0].astype(F32), norm_gain).astype(BF)
    normed = lax.all_gather(normed, ("fs", "tp"), axis=0, tiled=True)
    rows = normed.shape[0] // fs
    proj = jnp.dot(normed, w_in, preferred_element_type=F32).astype(BF)
    parts = []
    at = 0
    for w in widths:
        parts.append(proj[:, at : at + w])
        at += w
    gv, wq, gq, gk, wk, wv, low = parts
    up = quarter(decay_up, 1)
    logits = jnp.dot(low, up, preferred_element_type=F32) + quarter(decay_bias, 0)
    rate = jax.nn.log_sigmoid(logits) / SOFTMAX_TEMPER
    gh = gq.shape[1] // KEY_DIM
    nb = rows // SPAN
    q = gq.astype(F32).reshape(fs, nb, SPAN, gh, KEY_DIM) * KEY_DIM ** (-0.5)
    k = gk.astype(F32).reshape(fs, nb, SPAN, gh, KEY_DIM)
    v = gv.reshape(fs, nb, SPAN, gh, VALUE_DIM)
    tri = jnp.tril(jnp.ones((SPAN, SPAN), F32))
    within = jnp.cumsum(rate.reshape(fs, nb, SPAN, gh, KEY_DIM), axis=2)
    total = within[:, :, -1]
    q_dec = q * jnp.exp(within)
    k_dec = k * jnp.exp(-within)
    k_end = k * jnp.exp(total[:, :, None] - within)
    scores = dot("bnihd,bnjhd->bnhij", q_dec, k_dec)
    scores = jnp.where(tri > 0, scores, 0.0)
    local_out = dot("bnhij,bnjhe->bnihe", scores, v)
    update = dot("bnjhd,bnjhe->bnhde", k_end, v)
    state = jnp.zeros((fs, gh, KEY_DIM, VALUE_DIM), F32)
    entering = []
    for n in range(nb):
        entering.append(state)
        state = jnp.exp(total[:, n])[..., None] * state + update[:, n]
    entering = jnp.stack(entering, 1)
    span_decay = jnp.exp(jnp.sum(total, axis=1))
    packed = jnp.concatenate([state, span_decay[..., None]], -1)
    packed = lax.all_gather(packed, "sp")

    def step(position, subtotal):
        longer = packed[position, ..., -1:] * subtotal + packed[position, ..., :-1]
        return jnp.where(position < me, longer, subtotal)

    incoming = lax.fori_loop(0, sp - 1, step, jnp.zeros_like(state))
    before = jnp.cumsum(total, axis=1) - total
    entering = entering + jnp.exp(before)[..., None] * incoming[:, None]
    gla_out = local_out + dot("bnihd,bnhde->bnihe", q_dec, entering)
    gla_hidden = rms_rows(gla_out, head_gain).astype(BF).reshape(fs * rows, gh * VALUE_DIM)
    kvh = wk.shape[1] // HEAD_DIM
    per = heads // kvh
    wb = rows // WINDOW
    kv = jnp.concatenate([wk, wv], 1).reshape(fs, rows, -1)
    edge = lax.ppermute(kv[:, rows - WINDOW :], "sp", [(i, i + 1) for i in range(sp - 1)])
    band = jnp.concatenate([edge, kv], 1)
    band = jnp.stack([band[:, i * WINDOW : (i + 2) * WINDOW] for i in range(wb)], 1).reshape(
        fs, wb, 2 * WINDOW, 2, kvh, HEAD_DIM
    )
    qw = wq.reshape(fs, wb, WINDOW, kvh, per, HEAD_DIM)
    s = dot("bnqhgd,bnkhd->bnhgqk", qw, band[:, :, :, 0]) * HEAD_DIM ** (-0.5)
    distance = jnp.arange(WINDOW)[:, None] + WINDOW - jnp.arange(2 * WINDOW)[None, :]
    where = me * rows + jnp.arange(wb)[:, None, None] * WINDOW - WINDOW + jnp.arange(2 * WINDOW)
    valid = ((distance >= 0) & (distance < WINDOW))[None] & (where >= 0)
    s = jnp.where(valid[None, :, None, None], s, -1e30)
    sink = quarter(sink_logit, 0).reshape(1, 1, kvh, per, 1, 1)
    top = jnp.maximum(jnp.max(s, -1, keepdims=True), sink)
    e = jnp.exp(s - top)
    weights = (e / (jnp.sum(e, -1, keepdims=True) + jnp.exp(sink - top))).astype(BF)
    hidden = dot("bnhgqk,bnkhd->bnqhgd", weights, band[:, :, :, 1]).astype(BF)
    hidden = hidden.reshape(fs * rows, heads * HEAD_DIM)
    both = jnp.concatenate([gla_hidden, hidden], 1)
    part = jnp.einsum("rk,skn->rsn", both, w_out, preferred_element_type=F32)
    part = part.reshape(fs * rows, -1)
    mixed = lax.psum_scatter(part, ("fs", "tp"), scatter_dimension=0, tiled=True)
    return mixed.astype(BF)[None]


def solution(mesh):
    in_specs = (
        P("fs", ("sp", "tp"), None),
        P(),
        P("sp", "tp"),
        P("sp", "tp"),
        P("sp", "tp"),
        P("sp", None),
        P(None, "tp"),
        P("tp"),
        P(),
        P("sp", "tp"),
        P("sp", "tp"),
        P("sp", "tp"),
        P("tp"),
        P("tp", "sp"),
        P("tp", "sp"),
    )
    out_specs = P("fs", ("sp", "tp"), None)
    return jax.shard_map(
        per_device, mesh=mesh, in_specs=in_specs, out_specs=out_specs, check_vma=False
    )
```

profile of v0, /device:TPU:0, one launch (start us, length us, event | category | flops | bytes accessed | tf_op | source)
XLA Modules:
  0.0 219.8 jit_solution(4197163426944656206)
XLA Ops:
  6.5 0.0 copy-start
  6.5 0.9 copy.54
  7.5 1.1 constant_dynamic-slice_fusion.2
  8.6 1.1 constant_dynamic-slice_fusion.4
  9.7 1.0 constant_dynamic-slice_fusion.6
  10.7 0.0 copy-start.5
  10.7 0.0 copy-start.6
  10.7 1.1 concatenate.23
  11.8 0.0 all-gather.8.cloned.1.call-update
  11.8 0.0 all-gather.6.cloned.1.call-start
  11.9 0.2 fusion.9
  12.1 0.8 fusion.11
  12.9 0.0 all-gather.6.cloned.1.call-update
  12.9 0.0 all-gather.10.cloned.1.call-start
  13.0 1.0 constant_dynamic-slice_fusion
  14.0 0.7 pad_maximum_fusion
  14.7 0.0 all-gather.10.cloned.1.call-update
  14.7 0.0 reduce-scatter.2.cloned.1.call-start
  14.8 0.0 copy-done.5
  14.8 0.1 dynamic_slice.54
  14.9 0.1 dynamic_slice.55
  15.0 0.1 fusion.28
  15.1 54.4 %all-gather.8.cloned.1.call-done = bf16[2048,544]{1,0:T(8,128)(2,1)} async-done(((bf16[512,544]{1,0:T(8,128)(2,1)}), bf16[2048,544]{1,0:T(8,128)(2,1)}) %all-gather.8.cloned.1.call-update) | async-done | bytes 2228240 | tf_op jit(solution)/shard_map/all_gather | solution.py:70
  69.5 28.5 %all-gather.6.cloned.1.call-done = bf16[512,2048]{1,0:T(8,128)(2,1)} async-done(((bf16[64,2048]{1,0:T(8,128)(2,1)}), bf16[512,2048]{1,0:T(8,128)(2,1)}) %all-gather.6.cloned.1.call-update) | async-done | bytes 2097168 | tf_op jit(solution)/shard_map/all_gather | solution.py:75
  97.9 3.8 %convolution_convert_fusion = bf16[512,544]{0,1:T(8,128)(2,1)S(1)} fusion(bf16[512,2048]{1,0:T(8,128)(2,1)} %all-gather.6.cloned.1.call-done, bf16[2048,544]{1,0:T(8,128)(2,1)} %all-gather.8.cloned.1.call-done), kind=kOutput, calls=%fused_computation.5 | convolution fusion | flops 1141129216 | bytes 4882432 | tf_op jit(solution)/shard_map/dot_general | solution.py:77
  101.8 0.4 fusion.18
  102.2 0.1 copy.83
  102.3 0.2 fusion.38
  102.6 0.1 copy.63
  102.7 0.1 copy.85
  102.9 0.1 copy.55
  103.0 0.7 copy.100
  103.7 0.7 reshape.337
  104.4 0.1 copy.82
  104.5 4.0 %collective-permute-start = (bf16[4,128,128]{1,2,0:T(8,128)(2,1)}, bf16[4,128,128]{1,2,0:T(8,128)(2,1)}, u32[]{:S(2)}, u32[]{:S(2)}) collective-permute-start(bf16[4,128,128]{1,2,0:T(8,128)(2,1)} %bitcast.104), channel_id=1, source_target_pairs={{0,8},{8,16},{16,24},{1,9},{9,17},{17,25},{2,10},{10,18},{18,26},{... | collective-permute-start | bytes 393224 | tf_op jit(solution)/shard_map/ppermute | solution.py:125
  108.6 0.2 convolution_bitcast_fusion
  108.9 0.1 bitcast_add_fusion.2
  109.0 0.1 fusion.19
  109.1 36.6 %all-gather = f32[16,1,64,129]{3,2,1,0:T(8,128)S(1)} all-gather(f32[4,1,64,129]{3,2,1,0:T(8,128)S(1)} %maximum_bitcast_fusion), channel_id=2, replica_groups=mesh['sp'=4,'fs'=4,'tp'=2] {'sp'}, dimensions={0}, use_global_device_ids=true | all-gather | bytes 660480 | tf_op jit(solution)/shard_map/all_gather | solution.py:110
  145.7 0.9 copy.65
  146.6 0.6 while.14
  146.6 0.1 fusion.50
  146.8 0.2 fusion.50
  147.0 0.2 fusion.50
  147.2 0.0 copy-start.4
  147.2 0.1 copy.66
  147.3 0.3 fusion.6
  147.6 0.4 multiply_reduce_fusion
  148.0 0.1 multiply_convert_fusion
  148.2 0.0 collective-permute-done
  148.2 0.9 copy_dynamic-update-slice_fusion.1
  149.2 0.4 fusion.37
  149.5 0.1 broadcast_maximum_fusion
  149.6 0.2 fusion.8
  149.8 0.1 exponential_add_fusion
  149.9 0.3 fusion.5
  150.2 0.2 copy.84
  150.4 0.1 reshape.349
  150.5 0.0 all-gather.10.cloned.1.call-done
  150.5 3.9 %fusion.13 = f32[512,4,512]{0,2,1:T(8,128)} fusion(bf16[4,256,512]{2,1,0:T(8,128)(2,1)} %bitcast.124, bf16[512,128]{1,0:T(8,128)(2,1)S(1)} %reshape.349, bf16[512,128]{1,0:T(8,128)(2,1)S(1)} %bitcast.125), kind=kOutput, calls=%fused_computation.29 | convolution fusion | flops 537395200 | bytes 5505024 | tf_op jit(solution)/shard_map/rk,skn->rsn/dot_general | solution.py:143
  154.5 5.4 %copy.76 = f32[512,2048]{1,0:T(8,128)} copy(f32[512,2048]{0,1:T(8,128)} %bitcast.112) | data formatting | bytes 8388608 | tf_op jit(solution)/shard_map/reshape | solution.py:144
  159.9 0.0 reduce-scatter.2.cloned.1.call-update
  159.9 51.5 %reduce-scatter.2.cloned.1.call-done = f32[64,2048]{1,0:T(8,128)} async-done(((f32[512,2048]{1,0:T(8,128)}), f32[64,2048]{1,0:T(8,128)}) %reduce-scatter.2.cloned.1.call-update) | async-done | bytes 524304 | tf_op jit(solution)/shard_map/reduce_scatter | solution.py:145
  211.5 1.8 convert_bitcast_fusion
  (32 shorter events, 0.4 us)
Async XLA Ops:
  6.5 95.3 %copy-start = (bf16[32,256]{1,0:T(8,128)(2,1)S(1)}, bf16[32,256]{1,0:T(8,128)(2,1)}, u32[]{:S(2)}) copy-start(bf16[32,256]{1,0:T(8,128)(2,1)} %param.23) | copy-start | bytes 49156
  6.5 5.4 %copy-start.1 = (bf16[1,64,2048]{2,1,0:T(8,128)(2,1)S(1)}, bf16[1,64,2048]{2,1,0:T(8,128)(2,1)}, u32[]{:S(2)}) copy-start(bf16[1,64,2048]{2,1,0:T(8,128)(2,1)} %param.17) | copy-start | bytes 786436
  6.5 62.9 %all-gather.8.cloned.1.call-start = ((), (), s32[]{:S(2)}) async-start(), calls=%async_computation.2 | async-start | bytes 3276800 | tf_op jit(solution)/shard_map/all_gather | solution.py:70
  6.5 5.5 %copy-start.3 = (f32[2048]{0:T(1024)S(1)}, f32[2048]{0:T(1024)}, u32[]{:S(2)}) copy-start(f32[2048]{0:T(1024)} %param.18) | copy-start | bytes 24580
  10.7 4.1 %copy-start.5 = (f32[256]{0:T(256)S(1)}, f32[256]{0:T(256)}, u32[]{:S(2)}) copy-start(f32[256]{0:T(256)} %param.24) | copy-start | bytes 3076
  10.7 4.2 %copy-start.6 = (f32[8]{0:T(128)S(1)}, f32[8]{0:T(128)}, u32[]{:S(2)}) copy-start(f32[8]{0:T(128)} %param.29) | copy-start | bytes 100
  11.8 86.1 %all-gather.6.cloned.1.call-start = ((), (), s32[]{:S(2)}) async-start(), calls=%async_computation.1 | async-start | bytes 2359296 | tf_op jit(solution)/shard_map/all_gather | solution.py:75
  12.9 137.6 %all-gather.10.cloned.1.call-start = ((), (), s32[]{:S(2)}) async-start(), calls=%async_computation.4 | async-start | bytes 1310720 | tf_op jit(solution)/shard_map/all_gather | solution.py:71
  14.7 196.8 %reduce-scatter.2.cloned.1.call-start = ((), (), s32[]{:S(2)}) async-start(), calls=%async_computation.3 | async-start | bytes 4718592 | tf_op jit(solution)/shard_map/reduce_scatter | solution.py:145
  104.5 43.7 %collective-permute-start = (bf16[4,128,128]{1,2,0:T(8,128)(2,1)}, bf16[4,128,128]{1,2,0:T(8,128)(2,1)}, u32[]{:S(2)}, u32[]{:S(2)}) collective-permute-start(bf16[4,128,128]{1,2,0:T(8,128)(2,1)} %bitcast.104), channel_id=1, source_target_pairs={{0,8},{8,16},{16,24},{1,9},{9,17},{17,25},{2,10},{10,18},{18,26},{... | collective-permute-start | bytes 393224 | tf_op jit(solution)/shard_map/ppermute | solution.py:125
  147.2 0.9 copy-start.4
  147.2 2.0 copy-start.2
Sparse Core Ops, SparseCore 0:
  12.0 57.4 all-gather.7
  71.4 26.5 all-gather.5
  99.5 42.4 all-gather.9
  160.1 51.3 reduce-scatter.1
where the time goes:
time: 220 us
  waiting for transfers between devices  134 us (61%)
  blocking collectives  36.6 us (17%)
  local copies, waits for them, and re-layouts  16.2 us (7%)
  between operations  13.5 us (6%)
  matrix products  9.71 us (4%)
  other arithmetic  5.13 us (2%)
  starting transfers between devices  4.18 us (2%)
    all_gather x1, waiting for transfers between devices, per_device(): w_in = lax.all_gather(jnp.concatenate(maps, 1), 'sp', axis=0, tiled=True)  54.4 us
    reduce_scatter x1, waiting for transfers between devices, per_device(): lax.psum_scatter(part, ('fs', 'tp'), scatter_dimension=0, tiled=True)  51.5 us
    all_gather x1, blocking collectives, per_device(): packed = lax.all_gather(packed, 'sp')  36.6 us
    all_gather x1, waiting for transfers between devices, per_device(): normed = lax.all_gather(normed, ('fs', 'tp'), axis=0, tiled=True)  28.5 us
    reshape x1, local copies, waits for them, and re-layouts, per_device(): part = part.reshape(fs * rows, -1)  5.43 us
  transfers between devices with their start and end apart: 5, of which 3 were waited for; matrix products, arithmetic and copies ran while one was open for 7% of the time, Pallas kernels for 0%

commit v1 on v0

--- a/solution.py
+++ b/solution.py
@@ -72,7 +72,10 @@
         jnp.concatenate([quarter(gla_output_weight, 0), quarter(window_output_weight, 0)], 0), "sp"
     )
     normed = rms_rows(tokens[0].astype(F32), norm_gain).astype(BF)
-    normed = lax.all_gather(normed, ("fs", "tp"), axis=0, tiled=True)
+    normed = jnp.concatenate(
+        lax.all_to_all(jnp.stack([normed] * lax.axis_size(("fs", "tp"))), ("fs", "tp"), 0, 0),
+        axis=0,
+    )
     rows = normed.shape[0] // fs
     proj = jnp.dot(normed, w_in, preferred_element_type=F32).astype(BF)
     parts = []

time: 220 us -> 190 us (0.86)
  waiting for transfers between devices: 134 us -> 99.8 us
  starting transfers between devices: 4.18 us -> 7.76 us
    all_gather x1, waiting for transfers between devices: 54.4 us -> 23.8 us  [per_device(): w_in = lax.all_gather(jnp.concatenate(maps, 1), 'sp', axis=0, tiled=True)]
    all_gather x1 -> x0, waiting for transfers between devices: 28.5 us -> none  [per_device(): normed = lax.all_gather(normed, ('fs', 'tp'), axis=0, tiled=True)]
    all_to_all x0 -> x1, waiting for transfers between devices: none -> 24.5 us  [per_device(): lax.all_to_all(jnp.stack([normed] * lax.axis_size(('fs', 'tp'))), ('fs',...]
    all_to_all x0 -> x1, starting transfers between devices: none -> 5.33 us  [per_device(): lax.all_to_all(jnp.stack([normed] * lax.axis_size(('fs', 'tp'))), ('fs',...]
  transfers between devices with their start and end apart: 5 -> 5, of which waited for: 3 -> 3; matrix products, arithmetic and copies ran while one was open for 7% -> 8% of each run, Pallas kernels for 0% -> 0%
where the time goes in v1:
time: 190 us; the launch traced here: 189 us
  waiting for transfers between devices  99.8 us (53%)
  blocking collectives  36.8 us (19%)
  local copies, waits for them, and re-layouts  17.8 us (9%)
  between operations  13.4 us (7%)
  matrix products  9.1 us (5%)
  starting transfers between devices  7.76 us (4%)
  other arithmetic  4.41 us (2%)
    reduce_scatter x1, waiting for transfers between devices, per_device(): lax.psum_scatter(part, ('fs', 'tp'), scatter_dimension=0, tiled=True)  51.5 us
    all_gather x1, blocking collectives, per_device(): packed = lax.all_gather(packed, 'sp')  36.8 us
    all_to_all x1, waiting for transfers between devices, per_device(): lax.all_to_all(jnp.stack([normed] * lax.axis_size(('fs', 'tp'))), ('fs',...  24.5 us
    all_gather x1, waiting for transfers between devices, per_device(): w_in = lax.all_gather(jnp.concatenate(maps, 1), 'sp', axis=0, tiled=True)  23.8 us
    reshape x1, local copies, waits for them, and re-layouts, per_device(): part = part.reshape(fs * rows, -1)  5.41 us
    all_to_all x1, starting transfers between devices, per_device(): lax.all_to_all(jnp.stack([normed] * lax.axis_size(('fs', 'tp'))), ('fs',...  5.33 us
    dot_general x1, matrix products, per_device(): part = jnp.einsum('rk,skn->rsn', both, w_out, preferred_element_type=F32)  3.93 us
  transfers between devices with their start and end apart: 5, of which 3 were waited for; matrix products, arithmetic and copies ran while one was open for 8% of the time, Pallas kernels for 0%

profile of v1, /device:TPU:0, one launch (start us, length us, event | category | flops | bytes accessed | tf_op | source)
XLA Modules:
  0.0 189.1 jit_solution(8577677740357880727)
XLA Ops:
  6.5 0.0 copy-start
  6.5 0.0 all-gather.5.cloned.1.call-start
  6.5 0.9 copy.54
  7.5 1.1 constant_dynamic-slice_fusion.2
  8.6 1.1 constant_dynamic-slice_fusion.4
  9.7 1.0 constant_dynamic-slice_fusion.6
  10.7 1.1 concatenate.23
  11.8 0.0 all-gather.5.cloned.1.call-update
  11.8 0.2 fusion.9
  12.0 0.0 copy-done.3
  12.0 0.1 fusion.13
  12.1 1.6 stack.7
  13.7 5.3 %all-to-all-start = ((bf16[8,64,2048]{2,1,0:T(8,128)(2,1)}), bf16[8,64,2048]{2,1,0:T(8,128)(2,1)S(1)}, u32[]{:S(2)}, u32[]{:S(2)}) async-start(bf16[8,64,2048]{2,1,0:T(8,128)(2,1)} %stack.7), calls=%async_computation | async-start | bytes 4194304 | tf_op jit(solution)/shard_map/all_to_all | solution.py:76
  19.1 0.0 all-gather.7.cloned.1.call-start
  19.1 1.0 constant_dynamic-slice_fusion
  20.1 0.7 pad_maximum_fusion
  20.8 0.0 all-gather.7.cloned.1.call-update
  20.8 0.0 reduce-scatter.2.cloned.1.call-start
  20.9 0.1 dynamic_slice.54
  21.0 0.1 dynamic_slice.55
  21.1 0.1 fusion.29
  21.2 24.5 %all-to-all-done = bf16[8,64,2048]{2,1,0:T(8,128)(2,1)S(1)} async-done(((bf16[8,64,2048]{2,1,0:T(8,128)(2,1)}), bf16[8,64,2048]{2,1,0:T(8,128)(2,1)S(1)}, u32[]{:S(2)}, u32[]{:S(2)}) %all-to-all-start) | async-done | bytes 2097184 | tf_op jit(solution)/shard_map/all_to_all | solution.py:76
  45.7 23.8 %all-gather.5.cloned.1.call-done = bf16[2048,544]{1,0:T(8,128)(2,1)} async-done(((bf16[512,544]{1,0:T(8,128)(2,1)}), bf16[2048,544]{1,0:T(8,128)(2,1)}) %all-gather.5.cloned.1.call-update) | async-done | bytes 2228240 | tf_op jit(solution)/shard_map/all_gather | solution.py:70
  69.4 3.2 %convolution_convert_fusion = bf16[512,544]{0,1:T(8,128)(2,1)S(1)} fusion(bf16[512,2048]{1,0:T(8,128)(2,1)S(1)} %bitcast.119, bf16[2048,544]{1,0:T(8,128)(2,1)} %all-gather.5.cloned.1.call-done), kind=kOutput, calls=%fused_computation.5 | convolution fusion | flops 1141129216 | bytes 4882432 | tf_op jit(solution)/shard_map/dot_general | solution.py:80
  72.7 0.4 fusion.19
  73.1 0.1 copy.83
  73.2 0.2 fusion.39
  73.5 0.1 copy.63
  73.6 0.1 copy.85
  73.8 0.1 copy.55
  73.9 0.7 copy.100
  74.6 0.7 reshape.355
  75.3 0.1 copy.82
  75.4 2.3 %collective-permute-start = (bf16[4,128,128]{1,2,0:T(8,128)(2,1)}, bf16[4,128,128]{1,2,0:T(8,128)(2,1)}, u32[]{:S(2)}, u32[]{:S(2)}) collective-permute-start(bf16[4,128,128]{1,2,0:T(8,128)(2,1)} %bitcast.103), channel_id=1, source_target_pairs={{0,8},{8,16},{16,24},{1,9},{9,17},{17,25},{2,10},{10,18},{18,26},{... | collective-permute-start | bytes 393224 | tf_op jit(solution)/shard_map/ppermute | solution.py:128
  77.8 0.2 convolution_bitcast_fusion
  78.1 0.1 bitcast_add_fusion.2
  78.2 0.1 fusion.20
  78.3 36.8 %all-gather = f32[16,1,64,129]{3,2,1,0:T(8,128)S(1)} all-gather(f32[4,1,64,129]{3,2,1,0:T(8,128)S(1)} %maximum_bitcast_fusion), channel_id=2, replica_groups=mesh['sp'=4,'fs'=4,'tp'=2] {'sp'}, dimensions={0}, use_global_device_ids=true | all-gather | bytes 660480 | tf_op jit(solution)/shard_map/all_gather | solution.py:113
  115.2 0.9 copy.65
  116.1 0.5 while.14
  116.1 0.1 fusion.51
  116.3 0.1 fusion.51
  116.4 0.1 fusion.51
  116.6 0.0 copy-start.4
  116.6 0.1 copy.66
  116.7 0.3 fusion.6
  117.1 0.4 multiply_reduce_fusion
  117.5 0.0 copy-done.4
  117.5 0.1 multiply_convert_fusion
  117.6 0.0 collective-permute-done
  117.6 0.9 copy_dynamic-update-slice_fusion.1
  118.6 0.4 fusion.38
  119.0 0.1 broadcast_maximum_fusion
  119.1 0.2 fusion.8
  119.2 0.1 exponential_add_fusion
  119.3 0.3 fusion.5
  119.6 0.2 copy.84
  119.8 0.1 reshape.366
  120.0 0.0 all-gather.7.cloned.1.call-done
  120.0 3.9 %fusion.14 = f32[512,4,512]{0,2,1:T(8,128)} fusion(bf16[4,256,512]{2,1,0:T(8,128)(2,1)} %bitcast.124, bf16[512,128]{1,0:T(8,128)(2,1)S(1)} %reshape.366, bf16[512,128]{1,0:T(8,128)(2,1)S(1)} %bitcast.125), kind=kOutput, calls=%fused_computation.30 | convolution fusion | flops 537395200 | bytes 5505024 | tf_op jit(solution)/shard_map/rk,skn->rsn/dot_general | solution.py:146
  123.9 5.4 %copy.76 = f32[512,2048]{1,0:T(8,128)} copy(f32[512,2048]{0,1:T(8,128)} %bitcast.111) | data formatting | bytes 8388608 | tf_op jit(solution)/shard_map/reshape | solution.py:147
  129.3 0.0 reduce-scatter.2.cloned.1.call-update
  129.3 51.5 %reduce-scatter.2.cloned.1.call-done = f32[64,2048]{1,0:T(8,128)} async-done(((f32[512,2048]{1,0:T(8,128)}), f32[64,2048]{1,0:T(8,128)}) %reduce-scatter.2.cloned.1.call-update) | async-done | bytes 524304 | tf_op jit(solution)/shard_map/reduce_scatter | solution.py:148
  180.8 1.8 convert_bitcast_fusion
  (32 shorter events, 0.4 us)
Async XLA Ops:
  6.5 66.2 %copy-start = (bf16[32,256]{1,0:T(8,128)(2,1)S(1)}, bf16[32,256]{1,0:T(8,128)(2,1)}, u32[]{:S(2)}) copy-start(bf16[32,256]{1,0:T(8,128)(2,1)} %param.23) | copy-start | bytes 49156
  6.5 5.3 %copy-start.1 = (bf16[1,64,2048]{2,1,0:T(8,128)(2,1)S(1)}, bf16[1,64,2048]{2,1,0:T(8,128)(2,1)}, u32[]{:S(2)}) copy-start(bf16[1,64,2048]{2,1,0:T(8,128)(2,1)} %param.17) | copy-start | bytes 786436
  6.5 62.9 %all-gather.5.cloned.1.call-start = ((), (), s32[]{:S(2)}) async-start(), calls=%async_computation.2 | async-start | bytes 3276800 | tf_op jit(solution)/shard_map/all_gather | solution.py:70
  6.5 5.4 %copy-start.3 = (f32[2048]{0:T(1024)S(1)}, f32[2048]{0:T(1024)}, u32[]{:S(2)}) copy-start(f32[2048]{0:T(1024)} %param.18) | copy-start | bytes 24580
  13.7 7.2 %copy-start.5 = (f32[256]{0:T(256)S(1)}, f32[256]{0:T(256)}, u32[]{:S(2)}) copy-start(f32[256]{0:T(256)} %param.24) | copy-start | bytes 3076
  13.7 7.3 %copy-start.6 = (f32[8]{0:T(128)S(1)}, f32[8]{0:T(128)}, u32[]{:S(2)}) copy-start(f32[8]{0:T(128)} %param.29) | copy-start | bytes 100
  13.7 31.9 %all-to-all-start = ((bf16[8,64,2048]{2,1,0:T(8,128)(2,1)}), bf16[8,64,2048]{2,1,0:T(8,128)(2,1)S(1)}, u32[]{:S(2)}, u32[]{:S(2)}) async-start(bf16[8,64,2048]{2,1,0:T(8,128)(2,1)} %stack.7), calls=%async_computation | async-start | bytes 4194304 | tf_op jit(solution)/shard_map/all_to_all | solution.py:76
  19.1 100.9 %all-gather.7.cloned.1.call-start = ((), (), s32[]{:S(2)}) async-start(), calls=%async_computation.4 | async-start | bytes 1310720 | tf_op jit(solution)/shard_map/all_gather | solution.py:71
  20.8 160.0 %reduce-scatter.2.cloned.1.call-start = ((), (), s32[]{:S(2)}) async-start(), calls=%async_computation.3 | async-start | bytes 4718592 | tf_op jit(solution)/shard_map/reduce_scatter | solution.py:148
  75.4 42.2 %collective-permute-start = (bf16[4,128,128]{1,2,0:T(8,128)(2,1)}, bf16[4,128,128]{1,2,0:T(8,128)(2,1)}, u32[]{:S(2)}, u32[]{:S(2)}) collective-permute-start(bf16[4,128,128]{1,2,0:T(8,128)(2,1)} %bitcast.103), channel_id=1, source_target_pairs={{0,8},{8,16},{16,24},{1,9},{9,17},{17,25},{2,10},{10,18},{18,26},{... | collective-permute-start | bytes 393224 | tf_op jit(solution)/shard_map/ppermute | solution.py:128
  116.6 0.9 copy-start.4
  116.6 2.0 %copy-start.2 = (bf16[4,128,2,64]{1,0,3,2:T(4,128)(2,1)S(1)}, bf16[4,128,2,64]{1,0,3,2:T(4,128)(2,1)}, u32[]{:S(2)}) copy-start(bf16[4,128,2,64]{1,0,3,2:T(4,128)(2,1)} %reshape.355) | copy-start | bytes 393220
Sparse Core Ops, SparseCore 0:
  11.9 57.4 all-gather.4
  71.0 42.8 all-gather.6
  129.5 51.3 reduce-scatter.1
